TPU v7x, 32 devices: a whole 2x2x4 slice. The times are simulated.
32 devices in a mesh: sp: 16 (over z, y, x), tp: 2 (over core).
Axes of the slice: x: 2, y: 2, z: 4, core: 2. Of those that a mesh axis runs over, the one named last changes fastest.
Arguments:
- tokens: bfloat16 [2048, 2048], P('sp', 'tp'), may hold values from -6 to 6
- pre_gain: float32 [2048], replicated, may hold values from 0.1 to 1.9
- w_query_stick: bfloat16 [2048, 1024], P(None, 'tp'), may hold values from -0.125 to 0.125
- w_key_stick: bfloat16 [2048, 1024], P(None, 'tp'), may hold values from -0.125 to 0.125
- w_value_stick: bfloat16 [2048, 1024], P(None, 'tp'), may hold values from -2 to 2, as said below
- w_query_window: bfloat16 [2048, 1024], P(None, 'tp'), may hold values from -20 to 20, as said below
- w_key_window: bfloat16 [2048, 512], P(None, 'tp'), may hold values from -1 to 1, as said below
- w_value_window: bfloat16 [2048, 512], P(None, 'tp'), may hold values from -2 to 2, as said below
- stick_bias: float32 [16], P('tp'), may hold values from -14 to -3
- sinks: float32 [16], P('tp'), may hold values from 2 to 6
- stick_gain: float32 [1024], P('tp'), may hold values from 0.1 to 1.9
- window_gain: float32 [1024], P('tp'), may hold values from 0.1 to 1.9
- w_out_stick: bfloat16 [1024, 2048], P('tp'), may hold values from -0.125 to 0.125
- w_out_window: bfloat16 [1024, 2048], P('tp'), may hold values from -0.125 to 0.125
- post_gain: float32 [2048], replicated, may hold values from 0.1 to 1.9
Outputs:
- layer_out: bfloat16 [2048, 2048], P(('sp', 'tp'))
Inputs may be any that keep to these rules, and one draw needn't show every extreme that they name: `w_key_window`: key weights of the windowed heads. `w_query_window`: query weights of the windowed heads. `w_value_stick`: value weights of the stick-breaking heads. `w_value_window`: value weights of the windowed heads.
All inputs are finite; a program needn't handle non-finite values.
Results may differ from a plain program's by a relative error of at most 0.018.
Values may be sent and summed in bfloat16 or wider, within the bound.
A program may use at most 64 MiB of HBM per device.

v0:
```python
import jax
import jax.numpy as jnp
from jax import lax
from jax.sharding import PartitionSpec as P

HEAD_DIM = 64
GROUP = 2
WINDOW = 128
SB_WIDTH = 1024
SW_WIDTH = 1024


epsilon = 1e-06


def passed_along(value, axis, steps):
    count = lax.axis_size(axis)
    initial, last = (max(0, -steps), min(count, count - steps))
    return lax.ppermute(value, axis, [(source, source + steps) for source in range(initial, last)])


def rounded(values):
    return lax.optimization_barrier(values.astype(jnp.bfloat16)).astype(jnp.float32)


def norm_rows(values, gain):
    stats = jnp.mean(values * values, axis=-1, keepdims=True)
    return values * lax.rsqrt(stats + epsilon) * gain


def stick_block(queries, key_pair, head_bias, key_mask, carried):
    result, logsum = carried
    head_count = queries.shape[1]
    key_rows = key_pair[0].reshape(key_pair.shape[1], head_count, HEAD_DIM)
    values = key_pair[1].reshape(key_pair.shape[1], head_count, HEAD_DIM)
    scores = jnp.einsum(
        "thd,shd->hts", queries, key_rows, preferred_element_type=jnp.float32
    ) * HEAD_DIM ** (-0.5)
    scores = scores + head_bias[:, None, None]
    usable = key_mask[None]
    log_keep = jnp.where(usable, jax.nn.log_sigmoid(-scores), 0.0)
    suffix = lax.cumsum(log_keep, axis=2, reverse=True) - log_keep
    stick_weights = jnp.where(
        usable, jnp.exp(jax.nn.log_sigmoid(scores) + suffix + logsum[:, :, None]), 0.0
    )
    stick_weights = stick_weights.astype(jnp.bfloat16)
    result = result + jnp.einsum(
        "hts,shd->htd", stick_weights, values, preferred_element_type=jnp.float32
    )
    logsum = logsum + jnp.sum(log_keep, axis=2)
    return (result, logsum)


def shards(
    tokens,
    pre_gain,
    w_query_stick,
    w_key_stick,
    w_value_stick,
    w_query_window,
    w_key_window,
    w_value_window,
    stick_bias,
    sinks,
    stick_gain,
    window_gain,
    w_out_stick,
    w_out_window,
    post_gain,
):
    gathered = lax.all_gather(tokens, "tp", axis=1, tiled=True)
    normed = norm_rows(gathered.astype(jnp.float32), pre_gain).astype(jnp.bfloat16)

    def project(weight):
        return jnp.dot(normed, weight, preferred_element_type=jnp.float32).astype(jnp.bfloat16)

    tok_rows = normed.shape[0]
    dev_index = lax.axis_index("sp")
    dev_count = lax.axis_size("sp")
    query_stick = project(w_query_stick)
    stick_heads = query_stick.shape[1] // HEAD_DIM
    queries = query_stick.reshape(tok_rows, stick_heads, HEAD_DIM)
    own_pair = jnp.stack([project(w_key_stick), project(w_value_stick)])
    pair_width = own_pair.shape[2]
    positions = jnp.arange(tok_rows, dtype=jnp.int32)
    initial = (
        jnp.zeros((stick_heads, tok_rows, HEAD_DIM), jnp.float32),
        jnp.zeros((stick_heads, tok_rows), jnp.float32),
    )
    collected = own_pair[None]
    for section_index in range(dev_count.bit_length() - 1):
        arrived = passed_along(collected, "sp", 2**section_index)
        collected = jnp.concatenate([arrived, collected], axis=0)
    per_group = min(dev_count, 8)
    group_count = dev_count // per_group
    grouped = collected.reshape(group_count, per_group, 2, tok_rows, pair_width)
    grouped = grouped.transpose(0, 2, 1, 3, 4).reshape(
        group_count, 2, per_group * tok_rows, pair_width
    )
    first_source = dev_index - (dev_count - 1)
    group_starts = (first_source + jnp.arange(group_count, dtype=jnp.int32) * per_group) * tok_rows
    query_pos = dev_index * tok_rows + positions
    span_offs = jnp.arange(per_group * tok_rows, dtype=jnp.int32)

    def visit_group(carried, inputs):
        key_pair, start_pos = inputs
        key_pos = start_pos + span_offs
        key_mask = (key_pos[None, :] >= 0) & (key_pos[None, :] < query_pos[:, None])
        return (stick_block(queries, key_pair, stick_bias, key_mask, carried), None)

    (stick_sum, _), _ = lax.scan(visit_group, initial, (grouped, group_starts), reverse=True)
    stick_out = (
        stick_sum.transpose(1, 0, 2).reshape(tok_rows, stick_heads * HEAD_DIM).astype(jnp.bfloat16)
    )
    query_window = project(w_query_window)
    window_pair = jnp.stack([project(w_key_window), project(w_value_window)])
    kv_heads = window_pair.shape[2] // HEAD_DIM
    previous = passed_along(window_pair, "sp", 1)
    extended = jnp.concatenate([previous, window_pair], axis=1)
    block_count = tok_rows // WINDOW
    extended = extended.reshape(2, block_count + 1, WINDOW, kv_heads, HEAD_DIM)
    banded = jnp.concatenate([extended[:, :-1], extended[:, 1:]], axis=2)
    q_blocks = query_window.reshape(block_count, WINDOW, kv_heads, GROUP, HEAD_DIM)
    logits = jnp.einsum(
        "nqhgd,nchd->nhgqc", q_blocks, banded[0], preferred_element_type=jnp.float32
    ) * HEAD_DIM ** (-0.5)
    query_offs = jnp.arange(WINDOW, dtype=jnp.int32)[:, None]
    key_offs = jnp.arange(2 * WINDOW, dtype=jnp.int32)[None, :]
    distance = query_offs + WINDOW - key_offs
    key_pos = (
        dev_index * tok_rows
        + jnp.arange(block_count, dtype=jnp.int32)[:, None] * WINDOW
        - WINDOW
        + key_offs
    )
    usable = ((distance >= 0) & (distance < WINDOW))[None] & (key_pos >= 0)[:, None, :]
    logits = jnp.where(usable[:, None, None], logits, -jnp.inf)
    sink_logit = sinks.reshape(kv_heads, GROUP)[None, :, :, None, None]
    row_top = jnp.maximum(jnp.max(logits, axis=-1, keepdims=True), sink_logit)
    weights_exp = jnp.exp(logits - row_top)
    normalizer = jnp.sum(weights_exp, axis=-1, keepdims=True) + jnp.exp(sink_logit - row_top)
    window_weights = (weights_exp / normalizer).astype(jnp.bfloat16)
    window_sum = jnp.einsum(
        "nhgqc,nchd->nqhgd", window_weights, banded[1], preferred_element_type=jnp.float32
    )
    window_out = window_sum.reshape(tok_rows, query_window.shape[1]).astype(jnp.bfloat16)
    stick_float = stick_out.astype(jnp.float32)
    window_float = window_out.astype(jnp.float32)
    squares = lax.psum(
        (jnp.sum(stick_float * stick_float, axis=1), jnp.sum(window_float * window_float, axis=1)),
        "tp",
    )
    stick_normed = (
        stick_float * lax.rsqrt(squares[0][:, None] / SB_WIDTH + epsilon) * stick_gain
    ).astype(jnp.bfloat16)
    window_normed = (
        window_float * lax.rsqrt(squares[1][:, None] / SW_WIDTH + epsilon) * window_gain
    ).astype(jnp.bfloat16)
    total = jnp.dot(stick_normed, w_out_stick, preferred_element_type=jnp.float32)
    combined = lax.psum_scatter(
        (total + jnp.dot(window_normed, w_out_window, preferred_element_type=jnp.float32)).astype(
            jnp.bfloat16
        ),
        "tp",
        scatter_dimension=0,
        tiled=True,
    ).astype(jnp.float32)
    combined = rounded(combined)
    return norm_rows(combined, post_gain).astype(jnp.bfloat16)


def solution(mesh):
    in_specs = (
        P("sp", "tp"),
        P(),
        P(None, "tp"),
        P(None, "tp"),
        P(None, "tp"),
        P(None, "tp"),
        P(None, "tp"),
        P(None, "tp"),
        P("tp"),
        P("tp"),
        P("tp"),
        P("tp"),
        P("tp", None),
        P("tp", None),
        P(),
    )
    out_specs = P(("sp", "tp"), None)
    return jax.shard_map(shards, mesh=mesh, in_specs=in_specs, out_specs=out_specs, check_vma=False)
```

profile of v0, /device:TPU:1, one launch (start us, length us, event | category | flops | bytes accessed | tf_op | source)
XLA Modules:
  0.0 288.9 jit_solution(16102651300037023315)
XLA Ops:
  6.5 2.5 all_gather.3
  9.3 2.2 fusion.23
  11.5 2.2 fusion.24
  13.7 4.3 %collective-permute-start = (bf16[1,2,128,512]{3,2,1,0:T(8,128)(2,1)S(1)}, bf16[1,2,128,512]{3,2,1,0:T(8,128)(2,1)S(1)}, u32[]{:S(2)}, u32[]{:S(2)}) collective-permute-start(bf16[1,2,128,512]{3,2,1,0:T(8,128)(2,1)S(1)} %maximum_bitcast_fusion), channel_id=1, source_target_pairs={{0,2},{2,4},{4,6},{6,8},{8,10},{10,12},{12,14},{14,16},{16,18},{18... | collective-permute-start | bytes 786440 | tf_op jit(solution)/shard_map/ppermute | solution.py:19
  18.0 5.3 %collective-permute-done = bf16[1,2,128,512]{3,2,1,0:T(8,128)(2,1)S(1)} collective-permute-done((bf16[1,2,128,512]{3,2,1,0:T(8,128)(2,1)S(1)}, bf16[1,2,128,512]{3,2,1,0:T(8,128)(2,1)S(1)}, u32[]{:S(2)}, u32[]{:S(2)}) %collective-permute-start) | collective-permute-done | bytes 262176 | tf_op jit(solution)/shard_map/ppermute | solution.py:19
  23.3 5.1 %collective-permute-start.1 = (bf16[2,2,128,512]{3,2,1,0:T(8,128)(2,1)S(1)}, bf16[2,2,128,512]{3,2,1,0:T(8,128)(2,1)S(1)}, u32[]{:S(2)}, u32[]{:S(2)}) collective-permute-start(bf16[2,2,128,512]{3,2,1,0:T(8,128)(2,1)S(1)} %pad_maximum_fusion.2), channel_id=1, source_target_pairs={{0,4},{2,6},{4,8},{6,10},{8,12},{10,14},{12,16},{14,18},{16,20},{1... | collective-permute-start | bytes 1572872 | tf_op jit(solution)/shard_map/ppermute | solution.py:19
  28.4 10.0 %collective-permute-done.1 = bf16[2,2,128,512]{3,2,1,0:T(8,128)(2,1)S(1)} collective-permute-done((bf16[2,2,128,512]{3,2,1,0:T(8,128)(2,1)S(1)}, bf16[2,2,128,512]{3,2,1,0:T(8,128)(2,1)S(1)}, u32[]{:S(2)}, u32[]{:S(2)}) %collective-permute-start.1) | collective-permute-done | bytes 524320 | tf_op jit(solution)/shard_map/ppermute | solution.py:19
  38.4 1.1 pad_maximum_fusion.1
  39.4 7.0 %collective-permute-start.2 = (bf16[4,2,128,512]{3,2,1,0:T(8,128)(2,1)}, bf16[4,2,128,512]{3,2,1,0:T(8,128)(2,1)}, u32[]{:S(2)}, u32[]{:S(2)}) collective-permute-start(bf16[4,2,128,512]{3,2,1,0:T(8,128)(2,1)} %pad_maximum_fusion.1), channel_id=1, source_target_pairs={{0,8},{2,10},{4,12},{6,14},{8,16},{10,18},{12,20},{14,22},{16,24},... | collective-permute-start | bytes 3145736 | tf_op jit(solution)/shard_map/ppermute | solution.py:19
  47.2 0.7 pad_maximum_fusion.4
  47.8 1.9 collective-permute-start.4
  49.8 3.1 %convolution_convert_fusion.1 = bf16[128,512]{1,0:T(8,128)(2,1)} fusion(bf16[2048,512]{1,0:T(8,128)(2,1)} %param.22, bf16[128,2048]{1,0:T(8,128)(2,1)} %copy-done.2, f32[2048]{0:T(1024)S(1)} %copy-done.19, f32[128]{0:T(128)S(1)} %add_rsqrt_fusion.3), kind=kOutput, calls=%fused_computation.44 | convolution fusion | flops 269549568 | bytes 2761216 | tf_op jit(solution)/shard_map/dot_general | solution.py:75
  52.8 13.3 %collective-permute-done.2 = bf16[4,2,128,512]{3,2,1,0:T(8,128)(2,1)} collective-permute-done((bf16[4,2,128,512]{3,2,1,0:T(8,128)(2,1)}, bf16[4,2,128,512]{3,2,1,0:T(8,128)(2,1)}, u32[]{:S(2)}, u32[]{:S(2)}) %collective-permute-start.2) | collective-permute-done | bytes 1048608 | tf_op jit(solution)/shard_map/ppermute | solution.py:19
  66.1 2.9 pad_maximum_fusion
  69.0 6.4 %collective-permute-start.3 = (bf16[8,2,128,512]{3,2,1,0:T(8,128)(2,1)}, bf16[8,2,128,512]{3,2,1,0:T(8,128)(2,1)}, u32[]{:S(2)}, u32[]{:S(2)}) collective-permute-start(bf16[8,2,128,512]{3,2,1,0:T(8,128)(2,1)} %pad_maximum_fusion), channel_id=1, source_target_pairs={{0,16},{2,18},{4,20},{6,22},{8,24},{10,26},{12,28},{14,30},{1,17},... | collective-permute-start | bytes 6291464 | tf_op jit(solution)/shard_map/ppermute | solution.py:19
  76.0 0.7 fusion.48
  76.7 1.7 copy.33
  78.4 0.7 copy.29
  79.7 0.9 maximum_maximum_fusion
  80.6 1.0 reshape.281
  81.7 1.9 fusion.58
  83.6 1.1 copy.41
  84.7 0.8 copy.42
  85.5 1.3 fusion.59
  87.1 2.4 multiply_reduce_fusion
  89.5 27.1 %collective-permute-done.3 = bf16[8,2,128,512]{3,2,1,0:T(8,128)(2,1)} collective-permute-done((bf16[8,2,128,512]{3,2,1,0:T(8,128)(2,1)}, bf16[8,2,128,512]{3,2,1,0:T(8,128)(2,1)}, u32[]{:S(2)}, u32[]{:S(2)}) %collective-permute-start.3) | collective-permute-done | bytes 2097184 | tf_op jit(solution)/shard_map/ppermute | solution.py:19
  116.6 3.1 %constant_dynamic-update-slice_fusion.4 = bf16[16,2,128,512]{3,2,1,0:T(8,128)(2,1)} fusion(bf16[8,2,128,512]{3,2,1,0:T(8,128)(2,1)} %collective-permute-done.3), kind=kLoop, calls=%fused_computation.96 | loop fusion | bytes 4194304
  119.7 2.3 constant_dynamic-update-slice_fusion.3
  122.0 0.8 constant_dynamic-update-slice_fusion.2
  122.8 0.7 constant_dynamic-update-slice_fusion.1
  123.5 0.7 constant_dynamic-update-slice_fusion
  124.2 7.6 %copy.28 = bf16[2,2,8,128,512]{3,2,4,1,0:T(8,128)(2,1)} copy(bf16[2,2,8,128,512]{4,3,1,2,0:T(8,128)(2,1)} %bitcast.4) | data formatting | bytes 8388608 | tf_op jit(solution)/shard_map/transpose | solution.py:97
  131.8 7.3 %reshape.265 = bf16[2,2,1024,512]{2,3,1,0:T(8,128)(2,1)} reshape(bf16[2,2,8,128,512]{3,2,4,1,0:T(8,128)(2,1)} %copy.28) | data formatting | bytes 8388608 | tf_op jit(solution)/shard_map/reshape | solution.py:97
  139.1 78.0 %while.17 = (s32[]{:T(128)}, f32[8,128,64]{1,2,0:T(8,128)S(1)}, f32[8,128]{1,0:T(8,128)S(1)}, s32[2]{0:T(128)S(1)}, bf16[2,2,1024,512]{2,3,1,0:T(8,128)(2,1)}, /...) while((s32[]{:T(128)}, f32[8,128,64]{1,2,0:T(8,128)S(1)}, ...), condition=%wide.region_5.6_spmd.clone, body=%wide.region_1.5_spmd.clone.sunk | while | flops 438766720 | bytes 71048560 | solution.py:111
  139.2 0.7 dynamic_slice.23
  139.8 0.7 iota_add_fusion.6
  140.5 0.7 broadcast_compare_fusion.2
  141.6 1.8 constant_dynamic-slice_fusion.3
  143.4 5.5 %fusion.90 = (f32[8,128]{1,0:T(8,128)S(1)}, f32[8,128,1024]{1,2,0:T(8,128)S(1)}, f32[8,1024,128]{2,1,0:T(8,128)}) fusion(f32[8]{0:T(128)S(1)} %get-tuple-element.353, pred[128,1024]{0,1:T(8,128)(4,1)S(1)} %compare_and_fusion.2, bf16[1024,8,64]{0,2,1:T(8,128)(2,1)S(1)} %bitcast.142, bf16[128,8,64]{0,2,1:T(8,128)(2,1)S(1)} %copy-done.10), kind=kOutput, calls=%fused_computation.33.clone.1 | convolution fusion | flops 145751040 | bytes 9703456 | tf_op jit(solution)/shard_map/while/body/eval_jaxpr/thd,shd->hts/dot_general | solution.py:36
  148.9 10.1 %fusion.91 = f32[8,128,8,128]{1,2,3,0:T(8,128)S(1)} fusion(f32[8,128,8,128]{1,3,2,0:T(8,128)S(1)} %bitcast.140), kind=kOutput, calls=%fused_computation.20.clone.1 | output fusion | flops 133169152 | bytes 8388608 | tf_op jit(solution)/shard_map/reduce-window.12
  158.9 2.0 copy-done.1
  161.5 1.4 reduce-window.28
  162.9 0.8 slice.84
  163.8 2.5 broadcast_add_fusion.2
  166.3 2.7 copy.48
  169.0 8.5 %fusion.93 = bf16[8,128,1024]{1,2,0:T(8,128)(2,1)S(1)} fusion(f32[8,128,8,128]{1,3,2,0:T(8,128)} %copy.48, f32[8,1024,128]{2,1,0:T(8,128)} %get-tuple-element.319, f32[8,128]{1,0:T(8,128)S(1)} %get-tuple-element.321, f32[8]{0:T(128)S(1)} %get-tuple-element.353, pred[128,1024]{0,1:T(8,128)(4,1)S(1)} %compare_and_fusion.2), kind=kLoop, calls=%fused_computation.9.clone.1 | loop fusion | flops 24117248 | bytes 10620960 | tf_op jit(solution)/shard_map/while/body/eval_jaxpr/convert_element_type | solution.py:46
  178.2 0.7 dynamic_slice.23
  178.8 0.7 iota_add_fusion.6
  179.5 0.7 broadcast_compare_fusion.2
  180.6 1.8 constant_dynamic-slice_fusion.3
  182.4 5.5 %fusion.90 = (f32[8,128]{1,0:T(8,128)S(1)}, f32[8,128,1024]{1,2,0:T(8,128)S(1)}, f32[8,1024,128]{2,1,0:T(8,128)}) fusion(f32[8]{0:T(128)S(1)} %get-tuple-element.353, pred[128,1024]{0,1:T(8,128)(4,1)S(1)} %compare_and_fusion.2, bf16[1024,8,64]{0,2,1:T(8,128)(2,1)S(1)} %bitcast.142, bf16[128,8,64]{0,2,1:T(8,128)(2,1)S(1)} %copy-done.10), kind=kOutput, calls=%fused_computation.33.clone.1 | convolution fusion | flops 145751040 | bytes 9703456 | tf_op jit(solution)/shard_map/while/body/eval_jaxpr/thd,shd->hts/dot_general | solution.py:36
  187.9 10.1 %fusion.91 = f32[8,128,8,128]{1,2,3,0:T(8,128)S(1)} fusion(f32[8,128,8,128]{1,3,2,0:T(8,128)S(1)} %bitcast.140), kind=kOutput, calls=%fused_computation.20.clone.1 | output fusion | flops 133169152 | bytes 8388608 | tf_op jit(solution)/shard_map/reduce-window.12
  198.0 2.0 copy-done.1
  200.5 1.4 reduce-window.28
  202.0 0.8 slice.84
  202.8 2.5 broadcast_add_fusion.2
  205.3 2.7 copy.48
  208.0 8.5 %fusion.93 = bf16[8,128,1024]{1,2,0:T(8,128)(2,1)S(1)} fusion(f32[8,128,8,128]{1,3,2,0:T(8,128)} %copy.48, f32[8,1024,128]{2,1,0:T(8,128)} %get-tuple-element.319, f32[8,128]{1,0:T(8,128)S(1)} %get-tuple-element.321, f32[8]{0:T(128)S(1)} %get-tuple-element.353, pred[128,1024]{0,1:T(8,128)(4,1)S(1)} %compare_and_fusion.2), kind=kLoop, calls=%fused_computation.9.clone.1 | loop fusion | flops 24117248 | bytes 10620960 | tf_op jit(solution)/shard_map/while/body/eval_jaxpr/convert_element_type | solution.py:46
  217.3 5.9 %all-reduce = (f32[128]{0:T(128)S(1)}, f32[128]{0:T(128)S(1)}) all-reduce(f32[128]{0:T(128)S(1)} %get-tuple-element.252, f32[128]{0:T(128)} %get-tuple-element.256), channel_id=1, replica_groups=mesh['sp'=16,'tp'=2] {'tp'}, use_global_device_ids=true, to_apply=%region_7.8 | all-reduce | flops 256 | bytes 2048 | tf_op jit(solution)/shard_map/psum | solution.py:149
  224.0 0.8 copy-done.4
  224.8 1.3 fusion.19
  226.1 53.0 %reduce-scatter.2.cloned.1.call-done = bf16[64,2048]{1,0:T(8,128)(2,1)} async-done(((bf16[128,2048]{1,0:T(8,128)(2,1)}), bf16[64,2048]{1,0:T(8,128)(2,1)}) %reduce-scatter.2.cloned.1.call-update) | async-done | bytes 262160 | tf_op jit(solution)/shard_map/reduce_scatter | solution.py:160
  279.1 1.1 fusion.31
  280.2 1.8 fusion.33
  (82 shorter events, 6.5 us)
Async XLA Ops:
  6.5 216.8 %copy-start = (bf16[512,2048]{1,0:T(8,128)(2,1)S(1)}, bf16[512,2048]{1,0:T(8,128)(2,1)}, u32[]{:S(2)}) copy-start(bf16[512,2048]{1,0:T(8,128)(2,1)} %param.29) | copy-start | bytes 6291460
  6.5 272.6 %reduce-scatter.2.cloned.1.call-start = ((), (), s32[]{:S(2)}) async-start(), calls=%async_computation.1 | async-start | bytes 786432 | tf_op jit(solution)/shard_map/reduce_scatter | solution.py:160
  9.1 37.7 %copy-start.2 = (bf16[128,2048]{1,0:T(8,128)(2,1)}, bf16[128,2048]{1,0:T(8,128)(2,1)S(1)}, u32[]{:S(2)}) copy-start(bf16[128,2048]{1,0:T(8,128)(2,1)S(1)} %all_gather.3) | copy-start | bytes 1572868
  9.2 37.2 %copy-start.17 = (bf16[2048,256]{1,0:T(8,128)(2,1)S(1)}, bf16[2048,256]{1,0:T(8,128)(2,1)}, u32[]{:S(2)}) copy-start(bf16[2048,256]{1,0:T(8,128)(2,1)} %param.23) | copy-start | bytes 3145732
  9.3 37.2 %copy-start.19 = (f32[2048]{0:T(1024)S(1)}, f32[2048]{0:T(1024)}, u32[]{:S(2)}) copy-start(f32[2048]{0:T(1024)} %param.18) | copy-start | bytes 24580
  11.5 16.9 %copy-start.5 = (bf16[1,128,512]{2,1,0:T(8,128)(2,1)}, bf16[1,128,512]{2,1,0:T(8,128)(2,1)S(1)}, u32[]{:S(2)}) copy-start(bf16[1,128,512]{2,1,0:T(8,128)(2,1)S(1)} %fusion.23) | copy-start | bytes 393220
  11.5 35.3 %copy-start.18 = (bf16[2048,256]{1,0:T(8,128)(2,1)S(1)}, bf16[2048,256]{1,0:T(8,128)(2,1)}, u32[]{:S(2)}) copy-start(bf16[2048,256]{1,0:T(8,128)(2,1)} %param.24) | copy-start | bytes 3145732
  13.7 14.7 %copy-start.7 = (bf16[1,128,512]{2,1,0:T(8,128)(2,1)}, bf16[1,128,512]{2,1,0:T(8,128)(2,1)S(1)}, u32[]{:S(2)}) copy-start(bf16[1,128,512]{2,1,0:T(8,128)(2,1)S(1)} %fusion.24) | copy-start | bytes 393220
  13.7 9.5 %collective-permute-start = (bf16[1,2,128,512]{3,2,1,0:T(8,128)(2,1)S(1)}, bf16[1,2,128,512]{3,2,1,0:T(8,128)(2,1)S(1)}, u32[]{:S(2)}, u32[]{:S(2)}) collective-permute-start(bf16[1,2,128,512]{3,2,1,0:T(8,128)(2,1)S(1)} %maximum_bitcast_fusion), channel_id=1, source_target_pairs={{0,2},{2,4},{4,6},{6,8},{8,10},{10,12},{12,14},{14,16},{16,18},{18... | collective-permute-start | bytes 786440 | tf_op jit(solution)/shard_map/ppermute | solution.py:19
  23.3 15.1 %collective-permute-start.1 = (bf16[2,2,128,512]{3,2,1,0:T(8,128)(2,1)S(1)}, bf16[2,2,128,512]{3,2,1,0:T(8,128)(2,1)S(1)}, u32[]{:S(2)}, u32[]{:S(2)}) collective-permute-start(bf16[2,2,128,512]{3,2,1,0:T(8,128)(2,1)S(1)} %pad_maximum_fusion.2), channel_id=1, source_target_pairs={{0,4},{2,6},{4,8},{6,10},{8,12},{10,14},{12,16},{14,18},{16,20},{1... | collective-permute-start | bytes 1572872 | tf_op jit(solution)/shard_map/ppermute | solution.py:19
  39.4 26.7 %collective-permute-start.2 = (bf16[4,2,128,512]{3,2,1,0:T(8,128)(2,1)}, bf16[4,2,128,512]{3,2,1,0:T(8,128)(2,1)}, u32[]{:S(2)}, u32[]{:S(2)}) collective-permute-start(bf16[4,2,128,512]{3,2,1,0:T(8,128)(2,1)} %pad_maximum_fusion.1), channel_id=1, source_target_pairs={{0,8},{2,10},{4,12},{6,14},{8,16},{10,18},{12,20},{14,22},{16,24},... | collective-permute-start | bytes 3145736 | tf_op jit(solution)/shard_map/ppermute | solution.py:19
  47.8 31.9 %collective-permute-start.4 = (bf16[2,128,256]{2,1,0:T(8,128)(2,1)}, bf16[2,128,256]{2,1,0:T(8,128)(2,1)}, u32[]{:S(2)}, u32[]{:S(2)}) collective-permute-start(bf16[2,128,256]{2,1,0:T(8,128)(2,1)} %pad_maximum_fusion.4), channel_id=1, source_target_pairs={{0,2},{2,4},{4,6},{6,8},{8,10},{10,12},{12,14},{14,16},{16,18},{18... | collective-permute-start | bytes 393224 | tf_op jit(solution)/shard_map/ppermute | solution.py:19
  49.8 25.7 %copy-start.3 = (bf16[128,2048]{1,0:T(8,128)(2,1)S(1)}, bf16[128,2048]{1,0:T(8,128)(2,1)}, u32[]{:S(2)}) copy-start(bf16[128,2048]{1,0:T(8,128)(2,1)} %copy-done.2) | copy-start | bytes 1572868
  49.8 25.7 %copy-start.16 = (bf16[2048,512]{1,0:T(8,128)(2,1)S(1)}, bf16[2048,512]{1,0:T(8,128)(2,1)}, u32[]{:S(2)}) copy-start(bf16[2048,512]{1,0:T(8,128)(2,1)} %param.19) | copy-start | bytes 6291460
  52.8 25.5 %copy-start.15 = (f32[8]{0:T(128)S(1)}, f32[8]{0:T(128)}, u32[]{:S(2)}) copy-start(f32[8]{0:T(128)} %param.26) | copy-start | bytes 100
  69.0 47.5 %collective-permute-start.3 = (bf16[8,2,128,512]{3,2,1,0:T(8,128)(2,1)}, bf16[8,2,128,512]{3,2,1,0:T(8,128)(2,1)}, u32[]{:S(2)}, u32[]{:S(2)}) collective-permute-start(bf16[8,2,128,512]{3,2,1,0:T(8,128)(2,1)} %pad_maximum_fusion), channel_id=1, source_target_pairs={{0,16},{2,18},{4,20},{6,22},{8,24},{10,26},{12,28},{14,30},{1,17},... | collective-permute-start | bytes 6291464 | tf_op jit(solution)/shard_map/ppermute | solution.py:19
  89.5 34.0 %copy-start.6 = (bf16[1,128,512]{2,1,0:T(8,128)(2,1)S(1)}, bf16[1,128,512]{2,1,0:T(8,128)(2,1)}, u32[]{:S(2)}) copy-start(bf16[1,128,512]{2,1,0:T(8,128)(2,1)} %copy-done.5) | copy-start | bytes 393220
  89.5 34.0 %copy-start.8 = (bf16[1,128,512]{2,1,0:T(8,128)(2,1)S(1)}, bf16[1,128,512]{2,1,0:T(8,128)(2,1)}, u32[]{:S(2)}) copy-start(bf16[1,128,512]{2,1,0:T(8,128)(2,1)} %copy-done.7) | copy-start | bytes 393220
  131.8 7.3 %copy-start.11 = (f32[8]{0:T(128)S(1)}, f32[8]{0:T(128)}, u32[]{:S(2)}) copy-start(f32[8]{0:T(128)} %param.25) | copy-start | bytes 100
  131.8 7.3 %copy-start.20 = (s32[2]{0:T(128)S(1)}, s32[2]{0:T(128)}, u32[]{:S(2)}) copy-start(s32[2]{0:T(128)} %add_multiply_fusion) | copy-start | bytes 28
  139.1 84.1 %copy-start.13 = (f32[512]{0:T(512)S(1)}, f32[512]{0:T(512)}, u32[]{:S(2)}) copy-start(f32[512]{0:T(512)} %param.27) | copy-start | bytes 6148
  141.6 1.8 copy-start.10
  158.9 2.0 copy-start.1
  169.0 9.1 %copy-start.21 = (s32[2]{0:T(128)S(1)}, s32[2]{0:T(128)}, u32[]{:S(2)}) copy-start(s32[2]{0:T(128)} %get-tuple-element.379) | copy-start | bytes 28 | tf_op jit(solution)/shard_map/while
  180.6 1.8 copy-start.10
  198.0 2.0 copy-start.1
  208.0 9.1 %copy-start.21 = (s32[2]{0:T(128)S(1)}, s32[2]{0:T(128)}, u32[]{:S(2)}) copy-start(s32[2]{0:T(128)} %get-tuple-element.379) | copy-start | bytes 28 | tf_op jit(solution)/shard_map/while
  217.2 6.6 %copy-start.9 = (f32[4,64,2,128]{3,1,2,0:T(8,128)S(1)}, f32[4,64,2,128]{3,1,2,0:T(8,128)}, u32[]{:S(2)}) copy-start(f32[4,64,2,128]{3,1,2,0:T(8,128)} %get-tuple-element.257) | copy-start | bytes 786436
  217.2 6.6 %copy-start.14 = (f32[512]{0:T(512)S(1)}, f32[512]{0:T(512)}, u32[]{:S(2)}) copy-start(f32[512]{0:T(512)} %param.28) | copy-start | bytes 6148
  223.2 1.6 copy-start.4
  223.3 56.9 %copy-start.12 = (f32[2048]{0:T(1024)S(1)}, f32[2048]{0:T(1024)}, u32[]{:S(2)}) copy-start(f32[2048]{0:T(1024)} %param.31) | copy-start | bytes 24580
Sparse Core Ops, SparseCore 0:
  226.2 52.8 reduce-scatter.1
where the time goes:
time: 290 us; the launch traced here: 289 us
  waiting for transfers between devices  109 us (38%)
  other arithmetic  59.9 us (21%)
  local copies, waits for them, and re-layouts  47.2 us (16%)
  matrix products  26.2 us (9%)
  starting transfers between devices  24.6 us (8%)
  between operations  13.7 us (5%)
  blocking collectives  8.39 us (3%)
    ppermute x5, waiting for transfers between devices, passed_along(): lax.ppermute(value, axis, [(source, source + steps) for source in range(i...  55.6 us
    reduce_scatter x1, waiting for transfers between devices, shards(): lax.psum_scatter((total + jnp.dot(window_normed, w_out_window, preferred_...  53 us
    ppermute x5, starting transfers between devices, passed_along(): lax.ppermute(value, axis, [(source, source + steps) for source in range(i...  24.6 us
    another operation x4, other arithmetic  23 us
    convert_element_type x2, other arithmetic, stick_block(): stick_weights = stick_weights.astype(jnp.bfloat16)  17.1 us
    dot_general x2, matrix products, stick_block(): jnp.einsum('thd,shd->hts', queries, key_rows, preferred_element_type=jnp....  11 us
    unnamed x44, local copies, waits for them, and re-layouts  9.68 us
    dot_general x6, matrix products, project(): jnp.dot(normed, weight, preferred_element_type=jnp.float32)  8.62 us
  transfers between devices with their start and end apart: 6, of which 5 were waited for; matrix products, arithmetic and copies ran while one was open for 7% of the time, Pallas kernels for 0%

commit v1 on v0

--- a/solution.py
+++ b/solution.py
@@ -1,16 +1,469 @@
+import functools
+
 import jax
 import jax.numpy as jnp
 from jax import lax
+from jax.experimental import pallas as pl
+from jax.experimental.pallas import tpu as pltpu
 from jax.sharding import PartitionSpec as P
 
 HEAD_DIM = 64
 GROUP = 2
 WINDOW = 128
-SB_WIDTH = 1024
-SW_WIDTH = 1024
-
-
-epsilon = 1e-06
+EPS = 1e-06
+LOG2E = 1.4426950408889634
+MESH = pl.DeviceIdType.MESH
+
+
+def dot(a, b):
+    return jnp.dot(a, b, preferred_element_type=jnp.float32)
+
+
+def dot_t(a, b):
+    return lax.dot_general(a, b, (((1,), (1,)), ((), ())), preferred_element_type=jnp.float32)
+
+
+def kernel(
+    n_sp,
+    tokens, pre_gain, wqs, wks, wvs, wqw, wkw, wvw, bias, sinks, sgain, wgain, wos, wow, post_gain,
+    out,
+    x, bias_buf, normed, vqs, vks, vvs, vqw, vkw, vvw, vos, vow,
+    kv_send, q_send, kv_all, q_all, q_pad, staged,
+    kvw, kvw_prev, w_out_buf, o_send, o_recv, s_out_buf,
+    sq_send, sq_recv, total_w, comb, c_send, c_recv,
+    w_sem, tok_sem, x_ss, x_rs, b_ss, b_rs, kv_ss, kv_rs, q_ss, q_rs, f_ss, f_rs,
+    p_ss, p_rs, o_ss, o_rs, sq_ss, sq_rs, c_ss, c_rs,
+):
+    bf = jnp.bfloat16
+    f32 = jnp.float32
+    s = lax.axis_index("sp")
+    t = lax.axis_index("tp")
+    other = 1 - t
+    rows, feat_half = tokens.shape
+    feats = 2 * feat_half
+    half = rows // 2
+    quarter = half // 2
+    hd = HEAD_DIM
+    heads = wqs.shape[1] // hd
+    kv_heads = wkw.shape[1] // hd
+    sw = wqs.shape[1]
+
+    loads = [
+        pltpu.make_async_copy(src, dst, w_sem.at[n])
+        for n, (src, dst) in enumerate(
+            [(wks, vks), (wvs, vvs), (wqs, vqs), (wkw, vkw), (wvw, vvw), (wqw, vqw), (wow, vow), (wos, vos)]
+        )
+    ]
+    l_ks, l_vs, l_qs, l_kw, l_vw, l_qw, l_ow, l_os = loads
+    tok_load = pltpu.make_async_copy(tokens, x.at[t], tok_sem)
+    tok_load.start()
+    for load in loads:
+        load.start()
+
+    row_id = lax.broadcasted_iota(jnp.int32, (heads, 128), 0)
+    bias_rows = jnp.zeros((heads, 128), f32)
+    for i in range(heads):
+        bias_rows = jnp.where(row_id == i, bias[i] * LOG2E, bias_rows)
+    bias_buf[t] = bias_rows
+
+    barrier = pltpu.get_barrier_semaphore()
+    me = s * 2 + t
+
+    def greet(k, carry):
+        peer = lax.rem(me + k, 2 * n_sp)
+        pl.semaphore_signal(
+            barrier, inc=1, device_id={"sp": peer // 2, "tp": lax.rem(peer, 2)}, device_id_type=MESH
+        )
+        return carry
+
+    lax.fori_loop(1, 2 * n_sp, greet, 0)
+    tok_load.wait()
+    pl.semaphore_wait(barrier, 2 * n_sp - 1)
+
+    def to_partner(src, dst, ss, rs):
+        return pltpu.make_async_remote_copy(
+            src_ref=src, dst_ref=dst, send_sem=ss, recv_sem=rs,
+            device_id={"sp": s, "tp": other}, device_id_type=MESH,
+        )
+
+    x_copy = to_partner(x.at[t], x.at[t], x_ss, x_rs)
+    b_copy = to_partner(bias_buf.at[t], bias_buf.at[t], b_ss, b_rs)
+    x_copy.start()
+    b_copy.start()
+    x_copy.wait_recv()
+
+    gain = pre_gain[...].reshape(1, feats)
+
+    def norm_step(n, carry):
+        part = pl.ds(pl.multiple_of(n * 32, 32), 32)
+        left = x[0, part, :].astype(f32)
+        right = x[1, part, :].astype(f32)
+        stats = (
+            jnp.sum(left * left, axis=1, keepdims=True) + jnp.sum(right * right, axis=1, keepdims=True)
+        ) * (1.0 / feats)
+        inv = lax.rsqrt(stats + EPS)
+        normed[part, :feat_half] = (left * inv * gain[:, :feat_half]).astype(bf)
+        normed[part, feat_half:] = (right * inv * gain[:, feat_half:]).astype(bf)
+        return carry
+
+    lax.fori_loop(0, rows // 32, norm_step, 0)
+
+    l_ks.wait()
+    keys = dot(normed[...], vks[...])
+    l_vs.wait()
+    values = dot(normed[...], vvs[...])
+    for i in range(heads):
+        cols = slice(i * hd, (i + 1) * hd)
+        packed = jnp.concatenate([keys[:, cols], values[:, cols]], axis=1).astype(bf)
+        kv_send[i] = packed.reshape(2, half, 2 * hd)
+
+    def scatter(send, slots, ss, rs):
+        def step(k, carry):
+            i = lax.rem(k // 2 + s, heads)
+            u = lax.rem(k, 2)
+            chip = t * heads + i
+            is_self = jnp.logical_and(chip == s, u == t)
+
+            @pl.when(is_self)
+            def _():
+                pltpu.make_async_copy(send.at[i, u], slots(u), rs.at[s]).start()
+
+            @pl.when(jnp.logical_not(is_self))
+            def _():
+                pltpu.make_async_remote_copy(
+                    src_ref=send.at[i, u], dst_ref=slots(u), send_sem=ss.at[i, u], recv_sem=rs.at[s],
+                    device_id={"sp": chip, "tp": u}, device_id_type=MESH,
+                ).start()
+
+            return carry
+
+        lax.fori_loop(0, 2 * heads, step, 0)
+
+    def scatter_done(send, slots, ss, rs):
+        def step(k, carry):
+            i = k // 2
+            u = lax.rem(k, 2)
+            chip = t * heads + i
+            is_self = jnp.logical_and(chip == s, u == t)
+
+            @pl.when(jnp.logical_not(is_self))
+            def _():
+                pltpu.make_async_remote_copy(
+                    src_ref=send.at[i, u], dst_ref=slots(u), send_sem=ss.at[i, u], recv_sem=rs.at[s],
+                    device_id={"sp": chip, "tp": u}, device_id_type=MESH,
+                ).wait_send()
+
+            return carry
+
+        lax.fori_loop(0, 2 * heads, step, 0)
+
+    kv_slot = lambda u: kv_all.at[s, u]
+    q_slot = lambda u: q_all.at[s]
+    scatter(kv_send, kv_slot, kv_ss, kv_rs)
+
+    l_qs.wait()
+    queries = dot(normed[...], vqs[...])
+    for i in range(heads):
+        cols = slice(i * hd, (i + 1) * hd)
+        for u in range(2):
+            top = queries[u * half : u * half + quarter, cols]
+            low = queries[u * half + quarter : (u + 1) * half, cols]
+            q_send[i, u] = jnp.concatenate([top, low], axis=1).astype(bf)
+    scatter(q_send, q_slot, q_ss, q_rs)
+
+    l_kw.wait()
+    kvw[:, : kv_heads * hd] = dot(normed[...], vkw[...]).astype(bf)
+    l_vw.wait()
+    kvw[:, kv_heads * hd :] = dot(normed[...], vvw[...]).astype(bf)
+    prev_copy = lambda to: pltpu.make_async_remote_copy(
+        src_ref=kvw, dst_ref=kvw_prev, send_sem=p_ss, recv_sem=p_rs,
+        device_id={"sp": to, "tp": t}, device_id_type=MESH,
+    )
+
+    @pl.when(s < n_sp - 1)
+    def _():
+        prev_copy(s + 1).start()
+
+    l_qw.wait()
+    qw = dot(normed[...], vqw[...])
+
+    @pl.when(s == 0)
+    def _():
+        kvw_prev[...] = jnp.zeros_like(kvw_prev)
+
+    @pl.when(s > 0)
+    def _():
+        prev_copy(s - 1).wait_recv()
+
+    def forward(k, carry):
+        src = n_sp - 1 - k
+        pltpu.make_async_remote_copy(
+            src_ref=kv_send.at[0, 0], dst_ref=kv_all.at[src, t], send_sem=kv_ss.at[0, 0],
+            recv_sem=kv_rs.at[src], device_id={"sp": s, "tp": other}, device_id_type=MESH,
+        ).wait_recv()
+        to_partner(kv_all.at[src, t], kv_all.at[src, t], f_ss.at[src], f_rs.at[src]).start()
+        return carry
+
+    def forward_arrived(k, carry):
+        to_partner(kv_all.at[k, other], kv_all.at[k, other], f_ss.at[k], f_rs.at[k]).wait_recv()
+        return carry
+
+    def forward_sent(k, carry):
+        to_partner(kv_all.at[k, t], kv_all.at[k, t], f_ss.at[k], f_rs.at[k]).wait_send()
+        return carry
+
+    two = 2 * rows
+    r_iota = lax.broadcasted_iota(jnp.int32, (two, two), 0)
+    c_iota = lax.broadcasted_iota(jnp.int32, (two, two), 1)
+    dist = lax.rem(r_iota, rows) + rows - c_iota
+    in_window = (dist >= 0) & (dist < WINDOW) & ((c_iota >= rows) | (s > 0))
+    first_rows = lax.broadcasted_iota(jnp.int32, (two, 1), 0) < rows
+    for g in range(kv_heads):
+        cols = slice(g * hd, (g + 1) * hd)
+        v_cols = slice((kv_heads + g) * hd, (kv_heads + g + 1) * hd)
+        kk = jnp.concatenate([kvw_prev[:, cols], kvw[:, cols]], axis=0)
+        vv = jnp.concatenate([kvw_prev[:, v_cols], kvw[:, v_cols]], axis=0)
+        base = g * GROUP * hd
+        qq = jnp.concatenate(
+            [qw[:, base : base + hd], qw[:, base + hd : base + 2 * hd]], axis=0
+        ).astype(bf)
+        logits = jnp.where(in_window, dot_t(qq, kk) * hd**-0.5, -jnp.inf)
+        sink = jnp.where(first_rows, sinks[GROUP * g], sinks[GROUP * g + 1])
+        top = jnp.maximum(jnp.max(logits, axis=1, keepdims=True), sink)
+        grown = jnp.exp(logits - top)
+        total = jnp.sum(grown, axis=1, keepdims=True) + jnp.exp(sink - top)
+        weights = (grown / total).astype(bf)
+        res = dot(weights, vv)
+        w_out_buf[:, base : base + 2 * hd] = jnp.concatenate([res[:rows], res[rows:]], axis=1).astype(bf)
+
+    wf = w_out_buf[...].astype(f32)
+    sq_send[0] = jnp.broadcast_to(jnp.sum(wf * wf, axis=1, keepdims=True), (rows, 128))
+
+    lax.fori_loop(0, n_sp, forward, 0)
+    sq_w = to_partner(sq_send.at[0], sq_recv.at[0], sq_ss.at[0], sq_rs.at[0])
+    sq_w.start()
+
+    def take_q(k, carry):
+        pltpu.make_async_remote_copy(
+            src_ref=q_send.at[0, 0], dst_ref=q_all.at[k], send_sem=q_ss.at[0, 0],
+            recv_sem=q_rs.at[k], device_id={"sp": s, "tp": other}, device_id_type=MESH,
+        ).wait_recv()
+        slab = q_all[k].astype(f32)
+        zero = jnp.zeros((quarter, hd), f32)
+        both = jnp.concatenate(
+            [
+                jnp.concatenate([slab[:, :hd], zero], axis=1),
+                jnp.concatenate([slab[:, hd:], zero], axis=1),
+            ],
+            axis=0,
+        )
+        q_pad[pl.ds(pl.multiple_of(k * half, half), half), :] = both.astype(bf)
+        return carry
+
+    lax.fori_loop(0, n_sp, take_q, 0)
+    lax.fori_loop(0, n_sp, forward_arrived, 0)
+    b_copy.wait_recv()
+    head_bias = bias_buf[s // heads, pl.ds(lax.rem(s, heads), 1), :][:, :1]
+
+    kt = 2 * rows
+    chunk = 4 * half
+    later = (
+        lax.broadcasted_iota(jnp.int32, (kt, kt), 0) > lax.broadcasted_iota(jnp.int32, (kt, kt), 1)
+    ).astype(bf)
+    row = lax.broadcasted_iota(jnp.int32, (chunk, kt), 0)
+    lane = lax.broadcasted_iota(jnp.int32, (chunk, kt), 1)
+    q_at = (row // half) * rows + t * half + lax.rem(row, half)
+    scale = LOG2E * hd**-0.5
+
+    def tile_of(n):
+        return kv_all[2 * n : 2 * n + 2].reshape(kt, 2 * hd)
+
+    owner = s // heads
+    slot = lax.rem(s, heads)
+    for qc in reversed(range(n_sp // 4)):
+        last = 2 * qc + 1
+        carry = jnp.zeros((chunk, 1), f32)
+        carries = {}
+        for n in range(last, -1, -1):
+            low = chunk // 2 if n == last else 0
+            qs = q_pad[qc * chunk + low : (qc + 1) * chunk, :]
+            z = dot_t(qs, tile_of(n)) * scale + head_bias
+            pos = jnp.maximum(z, 0.0)
+            neg = z - pos
+            soft = jnp.log2(1.0 + jnp.exp2(neg - pos))
+            drop = pos + soft
+            hold = neg - soft
+            if n >= last - 1:
+                usable = (lane + (n - 2 * qc) * kt < q_at)[low:]
+                drop = jnp.where(usable, drop, 0.0)
+                hold = jnp.where(usable, hold, -jnp.inf)
+            suffix = dot(drop.astype(bf), later)
+            staged[low:, n * kt : (n + 1) * kt] = hold - suffix
+            carries[n] = carry[low:]
+            step = suffix[:, :1] + drop[:, :1]
+            if low:
+                step = jnp.concatenate([jnp.zeros((low, 1), f32), step], axis=0)
+            carry = carry + step
+        acc = None
+        for n in range(last - 1, -1, -1):
+            weights = jnp.exp2(staged[:, n * kt : (n + 1) * kt] - carries[n]).astype(bf)
+            res = dot(weights, tile_of(n))
+            acc = res if acc is None else acc + res
+        low = chunk // 2
+        weights = jnp.exp2(staged[low:, last * kt : (last + 1) * kt] - carries[last]).astype(bf)
+        tail = dot(weights, tile_of(last))
+        acc = jnp.concatenate([acc[:low], acc[low:] + tail], axis=0)
+        for b in range(4):
+            top = acc[b * half : b * half + quarter, hd:]
+            bot = acc[b * half + quarter : (b + 1) * half, hd:]
+            o_send[qc * 4 + b] = jnp.concatenate([top, bot], axis=1).astype(bf)
+
+        def give(k, carry):
+            is_self = jnp.logical_and(k == s, t == owner)
+
+            @pl.when(is_self)
+            def _():
+                pltpu.make_async_copy(o_send.at[k], o_recv.at[slot, t], o_rs.at[slot, t]).start()
+
+            @pl.when(jnp.logical_not(is_self))
+            def _():
+                pltpu.make_async_remote_copy(
+                    src_ref=o_send.at[k], dst_ref=o_recv.at[slot, t], send_sem=o_ss.at[k],
+                    recv_sem=o_rs.at[slot, t], device_id={"sp": k, "tp": owner}, device_id_type=MESH,
+                ).start()
+
+            return carry
+
+        lax.fori_loop(qc * 4, qc * 4 + 4, give, 0)
+
+    l_ow.wait()
+    total_w[...] = dot((wf * wgain[...].reshape(1, sw)).astype(bf), vow[...])
+    sq_w.wait_recv()
+    sw_cols = 2.0 * sw
+    inv_w = lax.rsqrt((sq_send[0] + sq_recv[0])[:, :1] / sw_cols + EPS)
+
+    def take_o(k, carry):
+        pltpu.make_async_remote_copy(
+            src_ref=o_send.at[0], dst_ref=o_recv.at[k // 2, lax.rem(k, 2)], send_sem=o_ss.at[0],
+            recv_sem=o_rs.at[k // 2, lax.rem(k, 2)], device_id={"sp": s, "tp": other}, device_id_type=MESH,
+        ).wait_recv()
+        return carry
+
+    lax.fori_loop(0, 2 * heads, take_o, 0)
+    for j in range(heads // 2):
+        for u in range(2):
+            one = o_recv[2 * j, u].astype(f32)
+            two_ = o_recv[2 * j + 1, u].astype(f32)
+            s_out_buf[u * half : u * half + quarter, 2 * j * hd : 2 * (j + 1) * hd] = jnp.concatenate(
+                [one[:, :hd], two_[:, :hd]], axis=1
+            )
+            s_out_buf[u * half + quarter : (u + 1) * half, 2 * j * hd : 2 * (j + 1) * hd] = jnp.concatenate(
+                [one[:, hd:], two_[:, hd:]], axis=1
+            )
+    sf = s_out_buf[...]
+    sq_send[1] = jnp.broadcast_to(jnp.sum(sf * sf, axis=1, keepdims=True), (rows, 128))
+    gained = (sf * sgain[...].reshape(1, sw)).astype(bf)
+    sq_s = to_partner(sq_send.at[1], sq_recv.at[1], sq_ss.at[1], sq_rs.at[1])
+    sq_s.start()
+    l_os.wait()
+    n_cut = c_send.shape[0]
+    cut = feats // n_cut
+    for n in range(n_cut):
+        comb[:, n * cut : (n + 1) * cut] = dot(gained, vos[:, n * cut : (n + 1) * cut])
+    sq_s.wait_recv()
+    inv_s = lax.rsqrt((sq_send[1] + sq_recv[1])[:, :1] / sw_cols + EPS)
+    copies = []
+    theirs = pl.ds(pl.multiple_of(other * half, half), half)
+    mine = pl.ds(pl.multiple_of(t * half, half), half)
+    for n in range(n_cut):
+        cols = slice(n * cut, (n + 1) * cut)
+        comb[:, cols] = comb[:, cols] * inv_s + total_w[:, cols] * inv_w
+        c_send[n] = comb[theirs, cols].astype(bf)
+        copy = to_partner(c_send.at[n], c_recv.at[n], c_ss.at[n], c_rs.at[n])
+        copy.start()
+        copies.append(copy)
+    square = jnp.zeros((half, 1), f32)
+    for n in range(n_cut):
+        cols = slice(n * cut, (n + 1) * cut)
+        copies[n].wait_recv()
+        summed = (comb[mine, cols] + c_recv[n].astype(f32)).astype(bf).astype(f32)
+        total_w[:half, cols] = summed
+        square = square + jnp.sum(summed * summed, axis=1, keepdims=True)
+    inv = lax.rsqrt(square / feats + EPS)
+    out[...] = (total_w[:half, :] * inv * post_gain[...].reshape(1, feats)).astype(bf)
+
+    x_copy.wait_send()
+    b_copy.wait_send()
+    scatter_done(kv_send, kv_slot, kv_ss, kv_rs)
+    scatter_done(q_send, q_slot, q_ss, q_rs)
+    lax.fori_loop(0, n_sp, forward_sent, 0)
+
+    @pl.when(s < n_sp - 1)
+    def _():
+        prev_copy(s + 1).wait_send()
+
+    def gave(k, carry):
+        @pl.when(jnp.logical_not(jnp.logical_and(k == s, t == owner)))
+        def _():
+            pltpu.make_async_remote_copy(
+                src_ref=o_send.at[k], dst_ref=o_recv.at[slot, t], send_sem=o_ss.at[k],
+                recv_sem=o_rs.at[slot, t], device_id={"sp": k, "tp": owner}, device_id_type=MESH,
+            ).wait_send()
+
+        return carry
+
+    lax.fori_loop(0, n_sp, gave, 0)
+    sq_w.wait_send()
+    sq_s.wait_send()
+    for copy in copies:
+        copy.wait_send()
+
+
+def one_kernel(n_sp, *args):
+    tokens, pre_gain, wqs, wks, wvs, wqw, wkw, wvw, bias, sinks, sgain, wgain, wos, wow, post_gain = args
+    bf = jnp.bfloat16
+    f32 = jnp.float32
+    rows, feat_half = tokens.shape
+    feats = 2 * feat_half
+    half = rows // 2
+    hd = HEAD_DIM
+    heads = wqs.shape[1] // hd
+    sw = wqs.shape[1]
+    wide = 2 * hd
+    kvw_cols = wkw.shape[1] + wvw.shape[1]
+    assert 2 * heads == n_sp and rows == WINDOW
+    v = pltpu.VMEM
+    dma = pltpu.SemaphoreType.DMA
+    anywhere = pl.BlockSpec(memory_space=pl.ANY)
+    vmem = pl.BlockSpec(memory_space=pltpu.VMEM)
+    smem = pl.BlockSpec(memory_space=pltpu.SMEM)
+    n_cut = 4
+    scratch = [
+        v((2, rows, feat_half), bf), v((2, heads, 128), f32), v((rows, feats), bf),
+        v(wqs.shape, bf), v(wks.shape, bf), v(wvs.shape, bf), v(wqw.shape, bf), v(wkw.shape, bf),
+        v(wvw.shape, bf), v(wos.shape, bf), v(wow.shape, bf),
+        v((heads, 2, half, wide), bf), v((heads, 2, half // 2, wide), bf),
+        v((n_sp, 2, half, wide), bf), v((n_sp, half // 2, wide), bf),
+        v((n_sp * half, wide), bf), v((4 * half, n_sp * rows), f32),
+        v((rows, kvw_cols), bf), v((rows, kvw_cols), bf), v((rows, sw), bf),
+        v((n_sp, half // 2, wide), bf), v((heads, 2, half // 2, wide), bf), v((rows, sw), f32),
+        v((2, rows, 128), f32), v((2, rows, 128), f32), v((rows, feats), f32), v((rows, feats), f32),
+        v((n_cut, half, feats // n_cut), bf), v((n_cut, half, feats // n_cut), bf),
+        dma((8,)), dma, dma, dma, dma, dma, dma((heads, 2)), dma((n_sp,)), dma((heads, 2)), dma((n_sp,)),
+        dma((n_sp,)), dma((n_sp,)), dma, dma, dma((n_sp,)), dma((heads, 2)), dma((2,)), dma((2,)),
+        dma((n_cut,)), dma((n_cut,)),
+    ]
+    return pl.pallas_call(
+        functools.partial(kernel, n_sp),
+        out_shape=jax.ShapeDtypeStruct((half, feats), bf),
+        in_specs=[anywhere, vmem] + [anywhere] * 6 + [smem, smem, vmem, vmem, anywhere, anywhere, vmem],
+        out_specs=vmem,
+        scratch_shapes=scratch,
+        compiler_params=pltpu.CompilerParams(
+            collective_id=0, has_side_effects=True, vmem_limit_bytes=48 * 1024 * 1024
+        ),
+        name="layer",
+    )(*args)
 
 
 def passed_along(value, axis, steps):
@@ -25,7 +478,7 @@
 
 def norm_rows(values, gain):
     stats = jnp.mean(values * values, axis=-1, keepdims=True)
-    return values * lax.rsqrt(stats + epsilon) * gain
+    return values * lax.rsqrt(stats + EPS) * gain
 
 
 def stick_block(queries, key_pair, head_bias, key_mask, carried):
@@ -51,7 +504,7 @@
     return (result, logsum)
 
 
-def shards(
+def by_collectives(
     tokens,
     pre_gain,
     w_query_stick,
@@ -151,10 +604,10 @@
         "tp",
     )
     stick_normed = (
-        stick_float * lax.rsqrt(squares[0][:, None] / SB_WIDTH + epsilon) * stick_gain
+        stick_float * lax.rsqrt(squares[0][:, None] / (stick_gain.shape[0] * lax.axis_size("tp")) + EPS) * stick_gain
     ).astype(jnp.bfloat16)
     window_normed = (
-        window_float * lax.rsqrt(squares[1][:, None] / SW_WIDTH + epsilon) * window_gain
+        window_float * lax.rsqrt(squares[1][:, None] / (window_gain.shape[0] * lax.axis_size("tp")) + EPS) * window_gain
     ).astype(jnp.bfloat16)
     total = jnp.dot(stick_normed, w_out_stick, preferred_element_type=jnp.float32)
     combined = lax.psum_scatter(
@@ -187,5 +640,18 @@
         P("tp", None),
         P(),
     )
-    out_specs = P(("sp", "tp"), None)
-    return jax.shard_map(shards, mesh=mesh, in_specs=in_specs, out_specs=out_specs, check_vma=False)
+    n_sp, n_tp = mesh.shape["sp"], mesh.shape["tp"]
+
+    def shards(*args):
+        heads = args[2].shape[1] // HEAD_DIM
+        if n_tp == 2 and n_tp * heads == n_sp and args[0].shape[0] == WINDOW and n_sp % 4 == 0:
+            return one_kernel(n_sp, *args)
+        return by_collectives(*args)
+
+    return jax.shard_map(
+        shards,
+        mesh=mesh,
+        in_specs=in_specs,
+        out_specs=P(("sp", "tp"), None),
+        check_vma=False,
+    )

time: 290 us -> 48.2 us (0.17)
  waiting for transfers between devices: 109 us -> 0 us
  other arithmetic: 59.9 us -> 0 us
  Pallas kernels: 0 us -> 38 us
  local copies, waits for them, and re-layouts: 47.2 us -> 9.76 us
  matrix products: 26.2 us -> 0 us
  starting transfers between devices: 24.6 us -> 0 us
  between operations: 13.7 us -> 0.02 us
  blocking collectives: 8.39 us -> 0 us
    ppermute x5 -> x0, waiting for transfers between devices: 55.6 us -> none  [passed_along(): lax.ppermute(value, axis, [(source, source + steps) for source in range(i...]
    reduce_scatter x1 -> x0, waiting for transfers between devices: 53 us -> none  [shards(): lax.psum_scatter((total + jnp.dot(window_normed, w_out_window, preferred_...]
    pallas_call x0 -> x1, Pallas kernels: none -> 38 us  [one_kernel(): pl.pallas_call(functools.partial(kernel, n_sp), out_shape=jax.ShapeDtypeS...]
    another operation x7 -> x0, other arithmetic: 28.7 us -> none
    dot_general x14 -> x0, matrix products: 26.2 us -> none  [the longest x2 11 us: stick_block(): jnp.einsum('thd,shd->hts', queries, key_rows, preferred_element_type=jnp....]
    ppermute x5 -> x0, starting transfers between devices: 24.6 us -> none  [passed_along(): lax.ppermute(value, axis, [(source, source + steps) for source in range(i...]
    convert_element_type x5 -> x0, other arithmetic: 19.1 us -> none  [the longest x2 17.1 us: stick_block(): stick_weights = stick_weights.astype(jnp.bfloat16)]
    reshape x2 -> x0, local copies, waits for them, and re-layouts: 8.34 us -> none  [the longest x1 7.29 us: shards(): grouped.transpose(0, 2, 1, 3, 4)]
  transfers between devices with their start and end apart: 6 -> 0, of which waited for: 5 -> 0; matrix products, arithmetic and copies ran while one was open for 7% -> 0% of each run, Pallas kernels for 0% -> 0%
where the time goes in v1:
time: 48.2 us; the launch traced here: 47.8 us
  Pallas kernels  38 us (79%)
  local copies, waits for them, and re-layouts  9.76 us (20%)
    pallas_call x1, Pallas kernels, one_kernel(): pl.pallas_call(functools.partial(kernel, n_sp), out_shape=jax.ShapeDtypeS...  38 us
    unnamed x21, local copies, waits for them, and re-layouts  9.76 us

profile of v1, /device:TPU:1, one launch (start us, length us, event | category | flops | bytes accessed | tf_op | source)
XLA Modules:
  0.0 47.8 jit_solution(7466934817969112161)
XLA Ops:
  0.0 0.0 copy-start
  0.0 1.6 %copy-done = bf16[2048,512]{1,0:T(8,128)(2,1)S(1)} copy-done((bf16[2048,512]{1,0:T(8,128)(2,1)S(1)}, bf16[2048,512]{1,0:T(8,128)(2,1)}, u32[]{:S(2)}) %copy-start) | copy-done | bytes 2097176
  1.6 0.0 copy-start.1
  1.6 1.2 %copy-done.1 = bf16[2048,256]{1,0:T(8,128)(2,1)S(1)} copy-done((bf16[2048,256]{1,0:T(8,128)(2,1)S(1)}, bf16[2048,256]{1,0:T(8,128)(2,1)}, u32[]{:S(2)}) %copy-start.1) | copy-done | bytes 1048600
  2.8 0.0 copy-start.2
  2.8 1.2 %copy-done.2 = bf16[2048,256]{1,0:T(8,128)(2,1)S(1)} copy-done((bf16[2048,256]{1,0:T(8,128)(2,1)S(1)}, bf16[2048,256]{1,0:T(8,128)(2,1)}, u32[]{:S(2)}) %copy-start.2) | copy-done | bytes 1048600
  4.0 0.0 copy-start.3
  4.0 0.9 %copy-done.3 = bf16[128,1024]{1,0:T(8,128)(2,1)S(1)} copy-done((bf16[128,1024]{1,0:T(8,128)(2,1)S(1)}, bf16[128,1024]{1,0:T(8,128)(2,1)}, u32[]{:S(2)}) %copy-start.3) | copy-done | bytes 262168
  5.0 0.0 copy-start.4
  5.0 0.7 %copy-done.4 = f32[2048]{0:T(1024)S(1)} copy-done((f32[2048]{0:T(1024)S(1)}, f32[2048]{0:T(1024)}, u32[]{:S(2)}) %copy-start.4) | copy-done | bytes 8216
  5.7 0.0 copy-start.5
  5.7 0.7 %copy-done.5 = f32[2048]{0:T(1024)S(1)} copy-done((f32[2048]{0:T(1024)S(1)}, f32[2048]{0:T(1024)}, u32[]{:S(2)}) %copy-start.5) | copy-done | bytes 8216
  6.4 0.0 copy-start.6
  6.4 0.7 %copy-done.6 = f32[512]{0:T(512)S(1)} copy-done((f32[512]{0:T(512)S(1)}, f32[512]{0:T(512)}, u32[]{:S(2)}) %copy-start.6) | copy-done | bytes 2072
  7.1 0.0 copy-start.7
  7.1 0.7 %copy-done.7 = f32[512]{0:T(512)S(1)} copy-done((f32[512]{0:T(512)S(1)}, f32[512]{0:T(512)}, u32[]{:S(2)}) %copy-start.7) | copy-done | bytes 2072
  7.8 0.0 copy-start.8
  7.8 0.7 %copy-done.8 = f32[8]{0:T(128)S(1)} copy-done((f32[8]{0:T(128)S(1)}, f32[8]{0:T(128)}, u32[]{:S(2)}) %copy-start.8) | copy-done | bytes 56
  8.4 0.0 copy-start.9
  8.4 0.7 %copy-done.9 = f32[8]{0:T(128)S(1)} copy-done((f32[8]{0:T(128)S(1)}, f32[8]{0:T(128)}, u32[]{:S(2)}) %copy-start.9) | copy-done | bytes 56
  9.1 38.0 %layer.1 = bf16[64,2048]{1,0:T(8,128)(2,1)S(1)} custom-call(bf16[128,1024]{1,0:T(8,128)(2,1)S(1)} %copy-done.3, f32[2048]{0:T(1024)S(1)} %copy-done.4, bf16[2048,512]{1,0:T(8,128)(2,1)S(1)} %copy-done, bf16[2048,512]{1,0:T(8,128)(2,1)} %wks.1, bf16[2048,512]{1,0:T(8,128)(2,1)} %wvs.1, bf16[2048,512]{1,0:T(8,128)(2,1)} %wqw.1, ...), custom_call_target="tpu_custom_call" | custom-call | tf_op jit(solution)/shard_map/layer/pallas_call | solution.py:456
  47.1 0.7 %copy.17 = bf16[64,2048]{1,0:T(8,128)(2,1)} copy(bf16[64,2048]{1,0:T(8,128)(2,1)S(1)} %layer.1) | data formatting | bytes 524288
Async XLA Ops:
  0.0 1.6 %copy-start = (bf16[2048,512]{1,0:T(8,128)(2,1)S(1)}, bf16[2048,512]{1,0:T(8,128)(2,1)}, u32[]{:S(2)}) copy-start(bf16[2048,512]{1,0:T(8,128)(2,1)} %wqs.1) | copy-start | bytes 6291460
  1.6 1.2 %copy-start.1 = (bf16[2048,256]{1,0:T(8,128)(2,1)S(1)}, bf16[2048,256]{1,0:T(8,128)(2,1)}, u32[]{:S(2)}) copy-start(bf16[2048,256]{1,0:T(8,128)(2,1)} %wkw.1) | copy-start | bytes 3145732
  2.8 1.2 %copy-start.2 = (bf16[2048,256]{1,0:T(8,128)(2,1)S(1)}, bf16[2048,256]{1,0:T(8,128)(2,1)}, u32[]{:S(2)}) copy-start(bf16[2048,256]{1,0:T(8,128)(2,1)} %wvw.1) | copy-start | bytes 3145732
  4.0 0.9 %copy-start.3 = (bf16[128,1024]{1,0:T(8,128)(2,1)S(1)}, bf16[128,1024]{1,0:T(8,128)(2,1)}, u32[]{:S(2)}) copy-start(bf16[128,1024]{1,0:T(8,128)(2,1)} %tokens.1) | copy-start | bytes 786436
  5.0 0.7 %copy-start.4 = (f32[2048]{0:T(1024)S(1)}, f32[2048]{0:T(1024)}, u32[]{:S(2)}) copy-start(f32[2048]{0:T(1024)} %pre_gain.1) | copy-start | bytes 24580
  5.7 0.7 %copy-start.5 = (f32[2048]{0:T(1024)S(1)}, f32[2048]{0:T(1024)}, u32[]{:S(2)}) copy-start(f32[2048]{0:T(1024)} %post_gain.1) | copy-start | bytes 24580
  6.4 0.7 %copy-start.6 = (f32[512]{0:T(512)S(1)}, f32[512]{0:T(512)}, u32[]{:S(2)}) copy-start(f32[512]{0:T(512)} %sgain.1) | copy-start | bytes 6148
  7.1 0.7 %copy-start.7 = (f32[512]{0:T(512)S(1)}, f32[512]{0:T(512)}, u32[]{:S(2)}) copy-start(f32[512]{0:T(512)} %wgain.1) | copy-start | bytes 6148
  7.8 0.7 %copy-start.8 = (f32[8]{0:T(128)S(1)}, f32[8]{0:T(128)}, u32[]{:S(2)}) copy-start(f32[8]{0:T(128)} %bias.1) | copy-start | bytes 100
  8.4 0.7 %copy-start.9 = (f32[8]{0:T(128)S(1)}, f32[8]{0:T(128)}, u32[]{:S(2)}) copy-start(f32[8]{0:T(128)} %sinks.1) | copy-start | bytes 100

commit v2 on v1

--- a/solution.py
+++ b/solution.py
@@ -25,9 +25,9 @@
 
 def kernel(
     n_sp,
-    tokens, pre_gain, wqs, wks, wvs, wqw, wkw, wvw, bias, sinks, sgain, wgain, wos, wow, post_gain,
-    out,
-    x, bias_buf, normed, vqs, vks, vvs, vqw, vkw, vvw, vos, vow,
+    tokens, pre_gain_in, wqs, wks, wvs, wqw, wkw, wvw, bias_in, sinks_in, sgain_in, wgain_in, wos, wow,
+    post_gain_in, out,
+    pre_gain, bias, sinks, sgain, wgain, post_gain, x, bias_buf, normed, vqs, vks, vvs, vqw, vkw, vvw, vos, vow,
     kv_send, q_send, kv_all, q_all, q_pad, staged,
     kvw, kvw_prev, w_out_buf, o_send, o_recv, s_out_buf,
     sq_send, sq_recv, total_w, comb, c_send, c_recv,
@@ -51,17 +51,21 @@
     loads = [
         pltpu.make_async_copy(src, dst, w_sem.at[n])
         for n, (src, dst) in enumerate(
-            [(wks, vks), (wvs, vvs), (wqs, vqs), (wkw, vkw), (wvw, vvw), (wqw, vqw), (wow, vow), (wos, vos)]
+            [(wks, vks), (wvs, vvs), (wqs, vqs), (wkw, vkw), (wvw, vvw), (wqw, vqw), (wow, vow), (wos, vos),
+             (bias_in, bias), (pre_gain_in, pre_gain), (sinks_in, sinks), (sgain_in, sgain),
+             (wgain_in, wgain), (post_gain_in, post_gain)]
         )
     ]
-    l_ks, l_vs, l_qs, l_kw, l_vw, l_qw, l_ow, l_os = loads
+    l_ks, l_vs, l_qs, l_kw, l_vw, l_qw, l_ow, l_os, l_bias, *l_small = loads
     tok_load = pltpu.make_async_copy(tokens, x.at[t], tok_sem)
+    l_bias.start()
     tok_load.start()
-    for load in loads:
+    for load in l_small + loads[:8]:
         load.start()
 
     row_id = lax.broadcasted_iota(jnp.int32, (heads, 128), 0)
     bias_rows = jnp.zeros((heads, 128), f32)
+    l_bias.wait()
     for i in range(heads):
         bias_rows = jnp.where(row_id == i, bias[i] * LOG2E, bias_rows)
     bias_buf[t] = bias_rows
@@ -77,6 +81,8 @@
         return carry
 
     lax.fori_loop(1, 2 * n_sp, greet, 0)
+    for load in l_small:
+        load.wait()
     tok_load.wait()
     pl.semaphore_wait(barrier, 2 * n_sp - 1)
 
@@ -436,9 +442,10 @@
     dma = pltpu.SemaphoreType.DMA
     anywhere = pl.BlockSpec(memory_space=pl.ANY)
     vmem = pl.BlockSpec(memory_space=pltpu.VMEM)
-    smem = pl.BlockSpec(memory_space=pltpu.SMEM)
     n_cut = 4
     scratch = [
+        v(pre_gain.shape, f32), pltpu.SMEM(bias.shape, f32), pltpu.SMEM(sinks.shape, f32),
+        v(sgain.shape, f32), v(wgain.shape, f32), v(post_gain.shape, f32),
         v((2, rows, feat_half), bf), v((2, heads, 128), f32), v((rows, feats), bf),
         v(wqs.shape, bf), v(wks.shape, bf), v(wvs.shape, bf), v(wqw.shape, bf), v(wkw.shape, bf),
         v(wvw.shape, bf), v(wos.shape, bf), v(wow.shape, bf),
@@ -449,18 +456,18 @@
         v((n_sp, half // 2, wide), bf), v((heads, 2, half // 2, wide), bf), v((rows, sw), f32),
         v((2, rows, 128), f32), v((2, rows, 128), f32), v((rows, feats), f32), v((rows, feats), f32),
         v((n_cut, half, feats // n_cut), bf), v((n_cut, half, feats // n_cut), bf),
-        dma((8,)), dma, dma, dma, dma, dma, dma((heads, 2)), dma((n_sp,)), dma((heads, 2)), dma((n_sp,)),
+        dma((14,)), dma, dma, dma, dma, dma, dma((heads, 2)), dma((n_sp,)), dma((heads, 2)), dma((n_sp,)),
         dma((n_sp,)), dma((n_sp,)), dma, dma, dma((n_sp,)), dma((heads, 2)), dma((2,)), dma((2,)),
         dma((n_cut,)), dma((n_cut,)),
     ]
     return pl.pallas_call(
         functools.partial(kernel, n_sp),
         out_shape=jax.ShapeDtypeStruct((half, feats), bf),
-        in_specs=[anywhere, vmem] + [anywhere] * 6 + [smem, smem, vmem, vmem, anywhere, anywhere, vmem],
+        in_specs=[anywhere] * len(args),
         out_specs=vmem,
         scratch_shapes=scratch,
         compiler_params=pltpu.CompilerParams(
-            collective_id=0, has_side_effects=True, vmem_limit_bytes=48 * 1024 * 1024
+            collective_id=0, has_side_effects=True, vmem_limit_bytes=67043328
         ),
         name="layer",
     )(*args)

time: 48.2 us -> 42.1 us (0.87)
  local copies, waits for them, and re-layouts: 9.76 us -> 1.67 us
  Pallas kernels: 38 us -> 40.3 us
    unnamed x21 -> x1, local copies, waits for them, and re-layouts: 9.76 us -> 1.67 us
    pallas_call x1, Pallas kernels: 38 us -> 40.3 us  [one_kernel(): pl.pallas_call(functools.partial(kernel, n_sp), out_shape=jax.ShapeDtypeS...]
where the time goes in v2:
time: 42.1 us; the launch traced here: 41.9 us
  Pallas kernels  40.3 us (96%)
  local copies, waits for them, and re-layouts  1.67 us (4%)
    pallas_call x1, Pallas kernels, one_kernel(): pl.pallas_call(functools.partial(kernel, n_sp), out_shape=jax.ShapeDtypeS...  40.3 us
    unnamed x1, local copies, waits for them, and re-layouts  1.67 us

profile of v2, /device:TPU:1, one launch (start us, length us, event | category | flops | bytes accessed | tf_op | source)
XLA Modules:
  0.0 41.9 jit_solution(17292278774268474900)
XLA Ops:
  0.0 40.3 %layer.1 = bf16[64,2048]{1,0:T(8,128)(2,1)} custom-call(bf16[128,1024]{1,0:T(8,128)(2,1)} %tokens.1, f32[2048]{0:T(1024)} %pre_gain_in.1, bf16[2048,512]{1,0:T(8,128)(2,1)} %wqs.1, bf16[2048,512]{1,0:T(8,128)(2,1)} %wks.1, bf16[2048,512]{1,0:T(8,128)(2,1)} %wvs.1, bf16[2048,512]{1,0:T(8,128)(2,1)} %wqw.1, bf16[2048,256]{1,0:T(8,128)(2,1)} %wkw.1, ...), custom_call_target="tpu_custom_call" | custom-call | tf_op jit(solution)/shard_map/layer/pallas_call | solution.py:463
  40.3 1.7 %copy.17 = bf16[64,2048]{1,0:T(8,128)(2,1)} copy(bf16[64,2048]{1,0:T(8,128)(2,1)} %layer.1) | data formatting | bytes 524288

commit v3 on v2

--- a/solution.py
+++ b/solution.py
@@ -48,6 +48,18 @@
     kv_heads = wkw.shape[1] // hd
     sw = wqs.shape[1]
 
+    barrier = pltpu.get_barrier_semaphore()
+    me = s * 2 + t
+
+    def greet(k, carry):
+        peer = lax.rem(me + k, 2 * n_sp)
+        pl.semaphore_signal(
+            barrier, inc=1, device_id={"sp": peer // 2, "tp": lax.rem(peer, 2)}, device_id_type=MESH
+        )
+        return carry
+
+    lax.fori_loop(1, 2 * n_sp, greet, 0)
+
     loads = [
         pltpu.make_async_copy(src, dst, w_sem.at[n])
         for n, (src, dst) in enumerate(
@@ -70,17 +82,6 @@
         bias_rows = jnp.where(row_id == i, bias[i] * LOG2E, bias_rows)
     bias_buf[t] = bias_rows
 
-    barrier = pltpu.get_barrier_semaphore()
-    me = s * 2 + t
-
-    def greet(k, carry):
-        peer = lax.rem(me + k, 2 * n_sp)
-        pl.semaphore_signal(
-            barrier, inc=1, device_id={"sp": peer // 2, "tp": lax.rem(peer, 2)}, device_id_type=MESH
-        )
-        return carry
-
-    lax.fori_loop(1, 2 * n_sp, greet, 0)
     for load in l_small:
         load.wait()
     tok_load.wait()
@@ -143,7 +144,7 @@
 
             return carry
 
-        lax.fori_loop(0, 2 * heads, step, 0)
+        lax.fori_loop(0, 2 * heads, step, 0, unroll=True)
 
     def scatter_done(send, slots, ss, rs):
         def step(k, carry):
@@ -186,23 +187,11 @@
         device_id={"sp": to, "tp": t}, device_id_type=MESH,
     )
 
-    @pl.when(s < n_sp - 1)
-    def _():
-        prev_copy(s + 1).start()
-
     l_qw.wait()
     qw = dot(normed[...], vqw[...])
 
-    @pl.when(s == 0)
-    def _():
-        kvw_prev[...] = jnp.zeros_like(kvw_prev)
-
-    @pl.when(s > 0)
-    def _():
-        prev_copy(s - 1).wait_recv()
-
     def forward(k, carry):
-        src = n_sp - 1 - k
+        src = k
         pltpu.make_async_remote_copy(
             src_ref=kv_send.at[0, 0], dst_ref=kv_all.at[src, t], send_sem=kv_ss.at[0, 0],
             recv_sem=kv_rs.at[src], device_id={"sp": s, "tp": other}, device_id_type=MESH,
@@ -217,37 +206,6 @@
     def forward_sent(k, carry):
         to_partner(kv_all.at[k, t], kv_all.at[k, t], f_ss.at[k], f_rs.at[k]).wait_send()
         return carry
-
-    two = 2 * rows
-    r_iota = lax.broadcasted_iota(jnp.int32, (two, two), 0)
-    c_iota = lax.broadcasted_iota(jnp.int32, (two, two), 1)
-    dist = lax.rem(r_iota, rows) + rows - c_iota
-    in_window = (dist >= 0) & (dist < WINDOW) & ((c_iota >= rows) | (s > 0))
-    first_rows = lax.broadcasted_iota(jnp.int32, (two, 1), 0) < rows
-    for g in range(kv_heads):
-        cols = slice(g * hd, (g + 1) * hd)
-        v_cols = slice((kv_heads + g) * hd, (kv_heads + g + 1) * hd)
-        kk = jnp.concatenate([kvw_prev[:, cols], kvw[:, cols]], axis=0)
-        vv = jnp.concatenate([kvw_prev[:, v_cols], kvw[:, v_cols]], axis=0)
-        base = g * GROUP * hd
-        qq = jnp.concatenate(
-            [qw[:, base : base + hd], qw[:, base + hd : base + 2 * hd]], axis=0
-        ).astype(bf)
-        logits = jnp.where(in_window, dot_t(qq, kk) * hd**-0.5, -jnp.inf)
-        sink = jnp.where(first_rows, sinks[GROUP * g], sinks[GROUP * g + 1])
-        top = jnp.maximum(jnp.max(logits, axis=1, keepdims=True), sink)
-        grown = jnp.exp(logits - top)
-        total = jnp.sum(grown, axis=1, keepdims=True) + jnp.exp(sink - top)
-        weights = (grown / total).astype(bf)
-        res = dot(weights, vv)
-        w_out_buf[:, base : base + 2 * hd] = jnp.concatenate([res[:rows], res[rows:]], axis=1).astype(bf)
-
-    wf = w_out_buf[...].astype(f32)
-    sq_send[0] = jnp.broadcast_to(jnp.sum(wf * wf, axis=1, keepdims=True), (rows, 128))
-
-    lax.fori_loop(0, n_sp, forward, 0)
-    sq_w = to_partner(sq_send.at[0], sq_recv.at[0], sq_ss.at[0], sq_rs.at[0])
-    sq_w.start()
 
     def take_q(k, carry):
         pltpu.make_async_remote_copy(
@@ -266,8 +224,6 @@
         q_pad[pl.ds(pl.multiple_of(k * half, half), half), :] = both.astype(bf)
         return carry
 
-    lax.fori_loop(0, n_sp, take_q, 0)
-    lax.fori_loop(0, n_sp, forward_arrived, 0)
     b_copy.wait_recv()
     head_bias = bias_buf[s // heads, pl.ds(lax.rem(s, heads), 1), :][:, :1]
 
@@ -286,7 +242,22 @@
 
     owner = s // heads
     slot = lax.rem(s, heads)
-    for qc in reversed(range(n_sp // 4)):
+    n_chunks = n_sp // 4
+
+    def arrive(qc):
+        lax.fori_loop(qc * 4, qc * 4 + 4, forward, 0, unroll=True)
+        lax.fori_loop(qc * 4, qc * 4 + 4, take_q, 0, unroll=True)
+
+    arrive(0)
+    for qc in range(n_chunks):
+        if qc + 1 < n_chunks:
+            arrive(qc + 1)
+        if qc + 2 == n_chunks:
+            @pl.when(s < n_sp - 1)
+            def _():
+                prev_copy(s + 1).start()
+
+        lax.fori_loop(qc * 4, qc * 4 + 4, forward_arrived, 0, unroll=True)
         last = 2 * qc + 1
         carry = jnp.zeros((chunk, 1), f32)
         carries = {}
@@ -341,6 +312,44 @@
             return carry
 
         lax.fori_loop(qc * 4, qc * 4 + 4, give, 0)
+
+    @pl.when(s == 0)
+    def _():
+        kvw_prev[...] = jnp.zeros_like(kvw_prev)
+
+    @pl.when(s > 0)
+    def _():
+        prev_copy(s - 1).wait_recv()
+
+    two = 2 * rows
+    r_iota = lax.broadcasted_iota(jnp.int32, (two, two), 0)
+    c_iota = lax.broadcasted_iota(jnp.int32, (two, two), 1)
+    dist = lax.rem(r_iota, rows) + rows - c_iota
+    in_window = (dist >= 0) & (dist < WINDOW) & ((c_iota >= rows) | (s > 0))
+    first_rows = lax.broadcasted_iota(jnp.int32, (two, 1), 0) < rows
+    for g in range(kv_heads):
+        cols = slice(g * hd, (g + 1) * hd)
+        v_cols = slice((kv_heads + g) * hd, (kv_heads + g + 1) * hd)
+        kk = jnp.concatenate([kvw_prev[:, cols], kvw[:, cols]], axis=0)
+        vv = jnp.concatenate([kvw_prev[:, v_cols], kvw[:, v_cols]], axis=0)
+        base = g * GROUP * hd
+        qq = jnp.concatenate(
+            [qw[:, base : base + hd], qw[:, base + hd : base + 2 * hd]], axis=0
+        ).astype(bf)
+        logits = jnp.where(in_window, dot_t(qq, kk) * hd**-0.5, -jnp.inf)
+        sink = jnp.where(first_rows, sinks[GROUP * g], sinks[GROUP * g + 1])
+        top = jnp.maximum(jnp.max(logits, axis=1, keepdims=True), sink)
+        grown = jnp.exp(logits - top)
+        total = jnp.sum(grown, axis=1, keepdims=True) + jnp.exp(sink - top)
+        weights = (grown / total).astype(bf)
+        res = dot(weights, vv)
+        w_out_buf[:, base : base + 2 * hd] = jnp.concatenate([res[:rows], res[rows:]], axis=1).astype(bf)
+
+    wf = w_out_buf[...].astype(f32)
+    sq_send[0] = jnp.broadcast_to(jnp.sum(wf * wf, axis=1, keepdims=True), (rows, 128))
+
+    sq_w = to_partner(sq_send.at[0], sq_recv.at[0], sq_ss.at[0], sq_rs.at[0])
+    sq_w.start()
 
     l_ow.wait()
     total_w[...] = dot((wf * wgain[...].reshape(1, sw)).astype(bf), vow[...])

time: 42.1 us -> 39 us (0.926)
  the two profiles are of different devices: /device:TPU:1 before, /device:TPU:9 now
where the time goes in v3:
time: 39 us; the launch traced here: 38.9 us
  Pallas kernels  37.2 us (95%)
  local copies, waits for them, and re-layouts  1.67 us (4%)
    pallas_call x1, Pallas kernels, one_kernel(): pl.pallas_call(functools.partial(kernel, n_sp), out_shape=jax.ShapeDtypeS...  37.2 us
    unnamed x1, local copies, waits for them, and re-layouts  1.67 us

profile of v3, /device:TPU:9, one launch (start us, length us, event | category | flops | bytes accessed | tf_op | source)
XLA Modules:
  0.0 38.9 jit_solution(14982573120027518377)
XLA Ops:
  0.0 37.2 %layer.1 = bf16[64,2048]{1,0:T(8,128)(2,1)} custom-call(bf16[128,1024]{1,0:T(8,128)(2,1)} %tokens.1, f32[2048]{0:T(1024)} %pre_gain_in.1, bf16[2048,512]{1,0:T(8,128)(2,1)} %wqs.1, bf16[2048,512]{1,0:T(8,128)(2,1)} %wks.1, bf16[2048,512]{1,0:T(8,128)(2,1)} %wvs.1, bf16[2048,512]{1,0:T(8,128)(2,1)} %wqw.1, bf16[2048,256]{1,0:T(8,128)(2,1)} %wkw.1, ...), custom_call_target="tpu_custom_call" | custom-call | tf_op jit(solution)/shard_map/layer/pallas_call | solution.py:472
  37.2 1.7 %copy.17 = bf16[64,2048]{1,0:T(8,128)(2,1)} copy(bf16[64,2048]{1,0:T(8,128)(2,1)} %layer.1) | data formatting | bytes 524288

commit v4 on v3

--- a/solution.py
+++ b/solution.py
@@ -28,10 +28,10 @@
     tokens, pre_gain_in, wqs, wks, wvs, wqw, wkw, wvw, bias_in, sinks_in, sgain_in, wgain_in, wos, wow,
     post_gain_in, out,
     pre_gain, bias, sinks, sgain, wgain, post_gain, x, bias_buf, normed, vqs, vks, vvs, vqw, vkw, vvw, vos, vow,
-    kv_send, q_send, kv_all, q_all, q_pad, staged,
+    kv_send, kv_all, q_pad, staged,
     kvw, kvw_prev, w_out_buf, o_send, o_recv, s_out_buf,
     sq_send, sq_recv, total_w, comb, c_send, c_recv,
-    w_sem, tok_sem, x_ss, x_rs, b_ss, b_rs, kv_ss, kv_rs, q_ss, q_rs, f_ss, f_rs,
+    w_sem, tok_sem, x_ss, x_rs, b_ss, b_rs, kv_ss, kv_rs, f_ss, f_rs,
     p_ss, p_rs, o_ss, o_rs, sq_ss, sq_rs, c_ss, c_rs,
 ):
     bf = jnp.bfloat16
@@ -122,7 +122,7 @@
     for i in range(heads):
         cols = slice(i * hd, (i + 1) * hd)
         packed = jnp.concatenate([keys[:, cols], values[:, cols]], axis=1).astype(bf)
-        kv_send[i] = packed.reshape(2, half, 2 * hd)
+        kv_send[i, :, :half] = packed.reshape(2, half, 2 * hd)
 
     def scatter(send, slots, ss, rs):
         def step(k, carry):
@@ -165,8 +165,6 @@
         lax.fori_loop(0, 2 * heads, step, 0)
 
     kv_slot = lambda u: kv_all.at[s, u]
-    q_slot = lambda u: q_all.at[s]
-    scatter(kv_send, kv_slot, kv_ss, kv_rs)
 
     l_qs.wait()
     queries = dot(normed[...], vqs[...])
@@ -175,8 +173,8 @@
         for u in range(2):
             top = queries[u * half : u * half + quarter, cols]
             low = queries[u * half + quarter : (u + 1) * half, cols]
-            q_send[i, u] = jnp.concatenate([top, low], axis=1).astype(bf)
-    scatter(q_send, q_slot, q_ss, q_rs)
+            kv_send[i, u, half:] = jnp.concatenate([top, low], axis=1).astype(bf)
+    scatter(kv_send, kv_slot, kv_ss, kv_rs)
 
     l_kw.wait()
     kvw[:, : kv_heads * hd] = dot(normed[...], vkw[...]).astype(bf)
@@ -196,23 +194,19 @@
             src_ref=kv_send.at[0, 0], dst_ref=kv_all.at[src, t], send_sem=kv_ss.at[0, 0],
             recv_sem=kv_rs.at[src], device_id={"sp": s, "tp": other}, device_id_type=MESH,
         ).wait_recv()
-        to_partner(kv_all.at[src, t], kv_all.at[src, t], f_ss.at[src], f_rs.at[src]).start()
+        to_partner(kv_all.at[src, t, :half], kv_all.at[src, t, :half], f_ss.at[src], f_rs.at[src]).start()
         return carry
 
     def forward_arrived(k, carry):
-        to_partner(kv_all.at[k, other], kv_all.at[k, other], f_ss.at[k], f_rs.at[k]).wait_recv()
+        to_partner(kv_all.at[k, other, :half], kv_all.at[k, other, :half], f_ss.at[k], f_rs.at[k]).wait_recv()
         return carry
 
     def forward_sent(k, carry):
-        to_partner(kv_all.at[k, t], kv_all.at[k, t], f_ss.at[k], f_rs.at[k]).wait_send()
+        to_partner(kv_all.at[k, t, :half], kv_all.at[k, t, :half], f_ss.at[k], f_rs.at[k]).wait_send()
         return carry
 
     def take_q(k, carry):
-        pltpu.make_async_remote_copy(
-            src_ref=q_send.at[0, 0], dst_ref=q_all.at[k], send_sem=q_ss.at[0, 0],
-            recv_sem=q_rs.at[k], device_id={"sp": s, "tp": other}, device_id_type=MESH,
-        ).wait_recv()
-        slab = q_all[k].astype(f32)
+        slab = kv_all[k, t, half:].astype(f32)
         zero = jnp.zeros((quarter, hd), f32)
         both = jnp.concatenate(
             [
@@ -238,7 +232,7 @@
     scale = LOG2E * hd**-0.5
 
     def tile_of(n):
-        return kv_all[2 * n : 2 * n + 2].reshape(kt, 2 * hd)
+        return kv_all[2 * n : 2 * n + 2, :, :half].reshape(kt, 2 * hd)
 
     owner = s // heads
     slot = lax.rem(s, heads)
@@ -410,7 +404,6 @@
     x_copy.wait_send()
     b_copy.wait_send()
     scatter_done(kv_send, kv_slot, kv_ss, kv_rs)
-    scatter_done(q_send, q_slot, q_ss, q_rs)
     lax.fori_loop(0, n_sp, forward_sent, 0)
 
     @pl.when(s < n_sp - 1)
@@ -458,14 +451,13 @@
         v((2, rows, feat_half), bf), v((2, heads, 128), f32), v((rows, feats), bf),
         v(wqs.shape, bf), v(wks.shape, bf), v(wvs.shape, bf), v(wqw.shape, bf), v(wkw.shape, bf),
         v(wvw.shape, bf), v(wos.shape, bf), v(wow.shape, bf),
-        v((heads, 2, half, wide), bf), v((heads, 2, half // 2, wide), bf),
-        v((n_sp, 2, half, wide), bf), v((n_sp, half // 2, wide), bf),
+        v((heads, 2, half + half // 2, wide), bf), v((n_sp, 2, half + half // 2, wide), bf),
         v((n_sp * half, wide), bf), v((4 * half, n_sp * rows), f32),
         v((rows, kvw_cols), bf), v((rows, kvw_cols), bf), v((rows, sw), bf),
         v((n_sp, half // 2, wide), bf), v((heads, 2, half // 2, wide), bf), v((rows, sw), f32),
         v((2, rows, 128), f32), v((2, rows, 128), f32), v((rows, feats), f32), v((rows, feats), f32),
         v((n_cut, half, feats // n_cut), bf), v((n_cut, half, feats // n_cut), bf),
-        dma((14,)), dma, dma, dma, dma, dma, dma((heads, 2)), dma((n_sp,)), dma((heads, 2)), dma((n_sp,)),
+        dma((14,)), dma, dma, dma, dma, dma, dma((heads, 2)), dma((n_sp,)),
         dma((n_sp,)), dma((n_sp,)), dma, dma, dma((n_sp,)), dma((heads, 2)), dma((2,)), dma((2,)),
         dma((n_cut,)), dma((n_cut,)),
     ]

time: 39 us -> 38.6 us (0.990)
  the two profiles are of different devices: /device:TPU:9 before, /device:TPU:17 now
where the time goes in v4:
time: 38.6 us; the launch traced here: 38.4 us
  Pallas kernels  36.8 us (95%)
  local copies, waits for them, and re-layouts  1.67 us (4%)
    pallas_call x1, Pallas kernels, one_kernel(): pl.pallas_call(functools.partial(kernel, n_sp), out_shape=jax.ShapeDtypeS...  36.8 us
    unnamed x1, local copies, waits for them, and re-layouts  1.67 us

profile of v4, /device:TPU:17, one launch (start us, length us, event | category | flops | bytes accessed | tf_op | source)
XLA Modules:
  0.0 38.4 jit_solution(9723494802979893596)
XLA Ops:
  0.0 36.8 %layer.1 = bf16[64,2048]{1,0:T(8,128)(2,1)} custom-call(bf16[128,1024]{1,0:T(8,128)(2,1)} %tokens.1, f32[2048]{0:T(1024)} %pre_gain_in.1, bf16[2048,512]{1,0:T(8,128)(2,1)} %wqs.1, bf16[2048,512]{1,0:T(8,128)(2,1)} %wks.1, bf16[2048,512]{1,0:T(8,128)(2,1)} %wvs.1, bf16[2048,512]{1,0:T(8,128)(2,1)} %wqw.1, bf16[2048,256]{1,0:T(8,128)(2,1)} %wkw.1, ...), custom_call_target="tpu_custom_call" | custom-call | tf_op jit(solution)/shard_map/layer/pallas_call | solution.py:464
  36.8 1.7 %copy.17 = bf16[64,2048]{1,0:T(8,128)(2,1)} copy(bf16[64,2048]{1,0:T(8,128)(2,1)} %layer.1) | data formatting | bytes 524288
